TPU v7x, 512 devices: a whole 4x4x16 slice. The times are simulated.
512 devices in a mesh: fs: 64 (over z, y), tp: 8 (over x, core).
Axes of the slice: x: 4, y: 4, z: 16, core: 2. Of those that a mesh axis runs over, the one named last changes fastest.
Arguments:
- tokens: bfloat16 [20480, 2048], P('fs'), may hold values from -6 to 6
- w_gate: bfloat16 [2048, 5632], P('fs', 'tp'), may hold values from -0.125 to 0.125
- w_up: bfloat16 [2048, 5632], P('fs', 'tp'), may hold values from -0.125 to 0.125
- w_down: bfloat16 [5632, 2048], P('tp', 'fs'), may hold values from -0.078125 to 0.078125
- w_mix_in: bfloat16 [2048, 1024], P('fs', 'tp'), may hold values from -0.125 to 0.125
- w_mix_out: bfloat16 [1024, 2048], P('tp', 'fs'), may hold values from -0.1875 to 0.1875
- pool_w: bfloat16 [8, 128, 128], P('tp'), may hold values from -0.5 to 0.5
- pool_scale: bfloat16 [1024], P('tp'), may hold values from 0.099609375 to 1.8984375
- norm_gains: float32 [6, 2048], replicated, may hold values from 0.1 to 1.9
Outputs:
- layer_out: bfloat16 [20480, 2048], P(('fs', 'tp'))
All inputs are finite; a program needn't handle non-finite values.
Results may differ from a plain program's by a relative error of at most 0.018.
Values may be sent and summed in bfloat16 or wider, within the bound.
No kernel may reach another device: no remote copies, remote signals or barrier semaphores. Data moves between devices by JAX's collectives and lax.ppermute only.
A program may use at most 64 MiB of HBM per device.

v0:
```python
import jax
import jax.numpy as jnp
from jax import lax
from jax.sharding import PartitionSpec as P

LEN = 64


def in_blocks(array, dim, peers):
    shape = array.shape
    tiles = array.reshape(*shape[:dim], peers, shape[dim] // peers, *shape[dim + 1 :])
    return jnp.moveaxis(tiles, dim, 0)


def sum_at_owner(array, axis, dim):
    peers = lax.axis_size(axis)
    tiles = lax.all_to_all(in_blocks(array, dim, peers), axis, 0, 0, tiled=True)
    return jnp.sum(tiles.astype(jnp.float32), axis=0)


def sent_to_all(array, axis):
    peers = lax.axis_size(axis)
    return lax.all_to_all(
        jnp.broadcast_to(array[None], (peers, *array.shape)), axis, 0, 0, tiled=True
    )


def in_order(tiles, dim):
    shape = list(tiles.shape[1:])
    shape[dim] *= tiles.shape[0]
    return jnp.moveaxis(tiles, 0, dim).reshape(shape)


def gathered_copies(array, axis, dim):
    tiles = sent_to_all(array, axis)
    return in_order(tiles, dim)


def rows_first(arrays, axis, dims):
    turned = [jnp.moveaxis(a, dim, 0) for a, dim in zip(arrays, dims)]
    both = jnp.concatenate([t.reshape(len(t), -1) for t in turned], axis=1)
    out, at, done = (lax.all_gather(both, axis, axis=0, tiled=True), 0, [])
    for t, dim in zip(turned, dims):
        share = out[:, at : at + t[0].size].reshape(-1, *t.shape[1:])
        done.append(jnp.moveaxis(share, 0, dim))
        at += t[0].size
    return tuple(done)


def sent_together(arrays, axis, dim, along):
    widths = [a.shape[along] for a in arrays]
    both = jnp.concatenate(arrays, axis=along)
    out = lax.all_gather(both, axis, axis=dim, tiled=True)
    return tuple(jnp.split(out, [sum(widths[:k]) for k in range(1, len(widths))], axis=along))


def rms_scale(values, gain):
    return values * lax.rsqrt(jnp.mean(values * values, axis=-1, keepdims=True) + 1e-06) * gain


def reduce_rows(left_rows, right_matrix):
    return sum_at_owner(
        jnp.dot(left_rows, right_matrix, preferred_element_type=jnp.float32).astype(jnp.bfloat16),
        "tp",
        0,
    )


def gather_rows(normed, project):
    return project(gathered_copies(normed, "tp", 0), jnp.int32(0))


def body(tokens, w_gate, w_up, w_down, w_mix_in, w_mix_out, pool_w, pool_scale, norm_gains):
    tp_size = lax.axis_size("tp")
    rows_all = tokens.shape[0]
    own_rows = rows_all // tp_size
    stream = tokens.astype(jnp.float32)
    normed = rms_scale(stream, norm_gains[0]).astype(jnp.bfloat16)
    down_full, mix_in_full, mix_out_full = rows_first(
        (w_down, w_mix_in, w_mix_out), "fs", (1, 0, 1)
    )
    gate_full, up_full = sent_together((w_gate, w_up), "fs", 0, 1)
    gate_first = jnp.dot(normed, gate_full, preferred_element_type=jnp.float32)
    up_first = jnp.dot(normed, up_full, preferred_element_type=jnp.float32)
    hidden = (jax.nn.silu(gate_first) * up_first).astype(jnp.bfloat16)
    stream_own = lax.dynamic_slice_in_dim(stream, lax.axis_index("tp") * own_rows, own_rows, 0)
    stream_own = stream_own + 0.5 * rms_scale(reduce_rows(hidden, down_full), norm_gains[1])
    normed = rms_scale(stream_own, norm_gains[2]).astype(jnp.bfloat16)

    def project_pool(part_rows, offset):
        return jnp.dot(part_rows, mix_in_full, preferred_element_type=jnp.float32).astype(
            jnp.bfloat16
        )

    pooled_in = gather_rows(normed, project_pool)
    groups_here = pool_w.shape[0]
    group_dim = pool_w.shape[1]
    values = pooled_in.astype(jnp.float32).reshape(rows_all // LEN, LEN, groups_here, group_dim)
    totals = jnp.cumsum(values, axis=1)
    position = jnp.arange(1, LEN + 1).astype(jnp.float32)[None, :, None, None]
    window_ids = (lax.axis_index("tp") * groups_here + jnp.arange(groups_here)) % 4
    average = jnp.zeros_like(values)
    for window_slot in range(4):
        window = 2 ** (1 + window_slot)
        lagged = jnp.pad(totals, ((0, 0), (window, 0), (0, 0), (0, 0)))[:, :LEN]
        candidate = (totals - lagged) / jnp.minimum(position, float(window))
        average = jnp.where((window_ids == window_slot)[None, None, :, None], candidate, average)
    deviation = (average - values).astype(jnp.bfloat16)
    regrouped = jnp.einsum("btgi,gio->btgo", deviation, pool_w, preferred_element_type=jnp.float32)
    regrouped = (
        regrouped.reshape(rows_all, groups_here * group_dim) * pool_scale.astype(jnp.float32)
    ).astype(jnp.bfloat16)
    stream_own = stream_own + rms_scale(reduce_rows(regrouped, mix_out_full), norm_gains[3])
    normed = rms_scale(stream_own, norm_gains[4]).astype(jnp.bfloat16)

    def project_ffn(part_rows, offset):
        gate_part = jnp.dot(part_rows, gate_full, preferred_element_type=jnp.float32)
        up_part = jnp.dot(part_rows, up_full, preferred_element_type=jnp.float32)
        return (jax.nn.silu(gate_part) * up_part).astype(jnp.bfloat16)

    hidden = gather_rows(normed, project_ffn)
    stream_own = stream_own + 0.5 * rms_scale(reduce_rows(hidden, down_full), norm_gains[5])
    return stream_own.astype(jnp.bfloat16)


def solution(mesh):
    in_specs = (
        P("fs", None),
        P("fs", "tp"),
        P("fs", "tp"),
        P("tp", "fs"),
        P("fs", "tp"),
        P("tp", "fs"),
        P("tp", None, None),
        P("tp"),
        P(),
    )
    out_specs = P(("fs", "tp"), None)
    return jax.shard_map(body, mesh=mesh, in_specs=in_specs, out_specs=out_specs, check_vma=False)
```

profile of v0, /device:TPU:1, one launch (start us, length us, event | category | flops | bytes accessed | tf_op | source)
XLA Modules:
  0.0 450.3 jit_solution(10392852320898855654)
XLA Ops:
  6.5 1.6 pad_maximum_fusion
  8.2 1.5 pad_maximum_fusion.1
  9.7 1.7 multiply_reduce_fusion
  11.4 1.1 fusion.49
  12.6 144.5 %all-gather.3.cloned.1.call-done = bf16[2048,1408]{1,0:T(8,128)(2,1)} async-done(((bf16[32,1408]{1,0:T(8,128)(2,1)}), bf16[2048,1408]{1,0:T(8,128)(2,1)}) %all-gather.3.cloned.1.call-update) | async-done | bytes 5767184 | tf_op jit(solution)/shard_map/all_gather | solution.py:53
  157.1 3.6 fusion.10
  160.7 139.5 %all-gather.5.cloned.1.call-done = bf16[2048,960]{1,0:T(8,128)(2,1)} async-done(((bf16[32,960]{1,0:T(8,128)(2,1)}), bf16[2048,960]{1,0:T(8,128)(2,1)}) %all-gather.5.cloned.1.call-update) | async-done | bytes 3932176 | tf_op jit(solution)/shard_map/all_gather | solution.py:42
  300.2 7.0 %fusion.12 = bf16[320,2048]{1,0:T(8,128)(2,1)} fusion(bf16[2048,960]{1,0:T(8,128)(2,1)} %all-gather.5.cloned.1.call-done, bf16[2048,1408]{1,0:T(8,128)(2,1)} %all-gather.3.cloned.1.call-done, f32[320,704]{1,0:T(8,128)S(1)} %fusion.10, f32[2048]{0:T(1024)S(1)} %bitcast.61, f32[320]{0:T(512)S(1)} %add_rsqrt_fusion, bf16[320,2048]{1,0:T(8,128)(2,1)S(1)} %copy-done.1), kind=kOutput, calls=%fused_computation.13 | convolution fusion | flops 1850122240 | bytes 9823488 | tf_op jit(solution)/shard_map/dot_general | solution.py:63
  307.2 13.9 %all-to-all-start = ((bf16[8,40,2048]{2,1,0:T(8,128)(2,1)}), bf16[8,40,2048]{2,1,0:T(8,128)(2,1)S(1)}, u32[]{:S(2)}, u32[]{:S(2)}) async-start(bf16[8,40,2048]{2,1,0:T(8,128)(2,1)} %bitcast.48), calls=%async_computation | async-start | bytes 2621440 | tf_op jit(solution)/shard_map/all_to_all | solution.py:17
  321.1 1.8 convert_element_type.82
  322.9 16.0 %all-to-all-done = bf16[8,40,2048]{2,1,0:T(8,128)(2,1)S(1)} async-done(((bf16[8,40,2048]{2,1,0:T(8,128)(2,1)}), bf16[8,40,2048]{2,1,0:T(8,128)(2,1)S(1)}, u32[]{:S(2)}, u32[]{:S(2)}) %all-to-all-start) | async-done | bytes 1310752 | tf_op jit(solution)/shard_map/all_to_all | solution.py:17
  338.9 0.2 convert_reduce_fusion.2
  339.1 0.1 multiply_reduce_fusion.5
  339.2 1.2 multiply_reduce_fusion.4
  340.6 1.2 broadcast_in_dim.60
  341.8 4.4 all-to-all-start.1
  346.3 17.8 %all-to-all-done.1 = bf16[8,40,2048]{2,1,0:T(8,128)(2,1)S(1)} async-done(((bf16[8,40,2048]{2,1,0:T(8,128)(2,1)}), bf16[8,40,2048]{2,1,0:T(8,128)(2,1)S(1)}, u32[]{:S(2)}, u32[]{:S(2)}) %all-to-all-start.1) | async-done | bytes 1310752 | tf_op jit(solution)/shard_map/all_to_all | solution.py:23
  364.0 1.8 convolution_convert_fusion.1
  366.0 1.7 subtract_convert_fusion
  367.7 0.2 fusion.43
  367.9 2.0 convolution_convert_fusion
  369.9 21.1 %all_to_all.25 = bf16[8,40,2048]{2,1,0:T(8,128)(2,1)S(1)} all-to-all(bf16[8,40,2048]{2,1,0:T(8,128)(2,1)S(1)} %bitcast.44), channel_id=1, replica_groups=mesh['fs'=64,'tp'=8] {'tp'}, dimensions={0} | all-to-all | bytes 2621440 | tf_op jit(solution)/shard_map/all_to_all | solution.py:17
  391.0 0.2 convert_reduce_fusion.1
  391.2 0.1 multiply_reduce_fusion.3
  391.3 0.2 multiply_reduce_fusion.2
  391.7 0.1 broadcast_in_dim.68
  391.8 21.2 %all_to_all.26 = bf16[8,40,2048]{2,1,0:T(8,128)(2,1)S(1)} all-to-all(bf16[8,40,2048]{2,1,0:T(8,128)(2,1)S(1)} %broadcast_in_dim.68), channel_id=1, replica_groups=mesh['fs'=64,'tp'=8] {'tp'}, dimensions={0} | all-to-all | bytes 2621440 | tf_op jit(solution)/shard_map/all_to_all | solution.py:23
  413.1 2.2 fusion.8
  415.3 5.9 %fusion.15 = bf16[320,2048]{1,0:T(8,128)(2,1)S(1)} fusion(bf16[2048,960]{1,0:T(8,128)(2,1)} %all-gather.5.cloned.1.call-done, bf16[320,2048]{1,0:T(8,128)(2,1)S(1)} %bitcast.50, bf16[2048,1408]{1,0:T(8,128)(2,1)} %all-gather.3.cloned.1.call-done, f32[320,704]{1,0:T(8,128)} %fusion.8), kind=kOutput, calls=%fused_computation.14 | convolution fusion | flops 1847500800 | bytes 9895936 | tf_op jit(solution)/shard_map/dot_general | solution.py:63
  421.2 21.2 %all_to_all.27 = bf16[8,40,2048]{2,1,0:T(8,128)(2,1)S(1)} all-to-all(bf16[8,40,2048]{2,1,0:T(8,128)(2,1)S(1)} %bitcast.51), channel_id=1, replica_groups=mesh['fs'=64,'tp'=8] {'tp'}, dimensions={0} | all-to-all | bytes 2621440 | tf_op jit(solution)/shard_map/all_to_all | solution.py:17
  442.4 0.2 convert_reduce_fusion
  442.7 0.8 add_convert_fusion
  (30 shorter events, 0.7 us)
Async XLA Ops:
  6.5 361.1 %copy-start = (bf16[1,128,128]{2,1,0:T(8,128)(2,1)S(1)}, bf16[1,128,128]{2,1,0:T(8,128)(2,1)}, u32[]{:S(2)}) copy-start(bf16[1,128,128]{2,1,0:T(8,128)(2,1)} %param.15) | copy-start | bytes 98308
  6.5 150.6 %all-gather.3.cloned.1.call-start = ((), (), s32[]{:S(2)}) async-start(), calls=%async_computation.5 | async-start | bytes 5857280 | tf_op jit(solution)/shard_map/all_gather | solution.py:53
  8.1 292.1 %all-gather.5.cloned.1.call-start = ((), (), s32[]{:S(2)}) async-start(), calls=%async_computation.6 | async-start | bytes 4259840 | tf_op jit(solution)/shard_map/all_gather | solution.py:42
  157.1 143.1 %copy-start.1 = (bf16[320,2048]{1,0:T(8,128)(2,1)S(1)}, bf16[320,2048]{1,0:T(8,128)(2,1)}, u32[]{:S(2)}) copy-start(bf16[320,2048]{1,0:T(8,128)(2,1)} %param.9) | copy-start | bytes 3932164
  307.2 31.7 %all-to-all-start = ((bf16[8,40,2048]{2,1,0:T(8,128)(2,1)}), bf16[8,40,2048]{2,1,0:T(8,128)(2,1)S(1)}, u32[]{:S(2)}, u32[]{:S(2)}) async-start(bf16[8,40,2048]{2,1,0:T(8,128)(2,1)} %bitcast.48), calls=%async_computation | async-start | bytes 2621440 | tf_op jit(solution)/shard_map/all_to_all | solution.py:17
  339.2 7.0 %copy-start.2 = (bf16[128]{0:T(256)(128)(2,1)S(1)}, bf16[128]{0:T(256)(128)(2,1)}, u32[]{:S(2)}) copy-start(bf16[128]{0:T(256)(128)(2,1)} %param.16) | copy-start | bytes 772
  341.8 22.2 %all-to-all-start.1 = ((bf16[8,40,2048]{2,1,0:T(8,128)(2,1)}), bf16[8,40,2048]{2,1,0:T(8,128)(2,1)S(1)}, u32[]{:S(2)}, u32[]{:S(2)}) async-start(bf16[8,40,2048]{2,1,0:T(8,128)(2,1)} %broadcast_in_dim.60), calls=%async_computation.1 | async-start | bytes 2621440 | tf_op jit(solution)/shard_map/all_to_all | solution.py:23
  367.9 45.2 %slice-start = ((s8[5767168]{0:T(1024)(128)(4,1)}), s8[4194304]{0:T(1024)(128)(4,1)S(1)}, s32[]{:S(2)}) async-start(s8[5767168]{0:T(1024)(128)(4,1)} %bitcast.62), calls=%async_computation.7 | async-start | bytes 8388608
  391.0 22.1 %slice-start.1 = ((s8[5767168]{0:T(1024)(128)(4,1)}), s8[1572864]{0:T(1024)(128)(4,1)S(1)}, s32[]{:S(2)}) async-start(s8[5767168]{0:T(1024)(128)(4,1)} %bitcast.62), calls=%async_computation.8 | async-start | bytes 3145728
Sparse Core Ops, SparseCore 0:
  10.3 146.7 all-gather.2
  160.0 140.1 all-gather.4
where the time goes:
time: 451 us; the launch traced here: 450 us
  waiting for transfers between devices  318 us (71%)
  blocking collectives  63.5 us (14%)
  matrix products  22.6 us (5%)
  starting transfers between devices  18.4 us (4%)
  between operations  13.6 us (3%)
  other arithmetic  11.9 us (3%)
    all_gather x1, waiting for transfers between devices, sent_together(): out = lax.all_gather(both, axis, axis=dim, tiled=True)  145 us
    all_gather x1, waiting for transfers between devices, rows_first(): out, at, done = (lax.all_gather(both, axis, axis=0, tiled=True), 0, [])  140 us
    all_to_all x2, blocking collectives, sum_at_owner(): tiles = lax.all_to_all(in_blocks(array, dim, peers), axis, 0, 0, tiled=True)  42.3 us
    all_to_all x1, blocking collectives, sent_to_all(): lax.all_to_all(jnp.broadcast_to(array[None], (peers, *array.shape)), axis...  21.2 us
    all_to_all x1, waiting for transfers between devices, sent_to_all(): lax.all_to_all(jnp.broadcast_to(array[None], (peers, *array.shape)), axis...  17.8 us
    all_to_all x1, waiting for transfers between devices, sum_at_owner(): tiles = lax.all_to_all(in_blocks(array, dim, peers), axis, 0, 0, tiled=True)  16 us
    dot_general x3, matrix products, reduce_rows(): jnp.dot(left_rows, right_matrix, preferred_element_type=jnp.float32)  14.8 us
    all_to_all x1, starting transfers between devices, sum_at_owner(): tiles = lax.all_to_all(in_blocks(array, dim, peers), axis, 0, 0, tiled=True)  13.9 us
  transfers between devices with their start and end apart: 4, of which 4 were waited for; matrix products, arithmetic and copies ran while one was open for 2% of the time, Pallas kernels for 0%

commit v1 on v0

--- a/solution.py
+++ b/solution.py
@@ -39,7 +39,13 @@
 def rows_first(arrays, axis, dims):
     turned = [jnp.moveaxis(a, dim, 0) for a, dim in zip(arrays, dims)]
     both = jnp.concatenate([t.reshape(len(t), -1) for t in turned], axis=1)
-    out, at, done = (lax.all_gather(both, axis, axis=0, tiled=True), 0, [])
+    out, at, done = (
+        jnp.concatenate(
+            lax.all_to_all(jnp.stack([both] * lax.axis_size(axis)), axis, 0, 0), axis=0
+        ),
+        0,
+        [],
+    )
     for t, dim in zip(turned, dims):
         share = out[:, at : at + t[0].size].reshape(-1, *t.shape[1:])
         done.append(jnp.moveaxis(share, 0, dim))

time: 451 us -> 405 us (0.90)
  waiting for transfers between devices: 318 us -> 259 us
  starting transfers between devices: 18.4 us -> 32.3 us
    all_gather x1 -> x0, waiting for transfers between devices: 140 us -> none  [rows_first(): out, at, done = (lax.all_gather(both, axis, axis=0, tiled=True), 0, [])]
    all_gather x1, waiting for transfers between devices: 145 us -> 226 us  [sent_together(): out = lax.all_gather(both, axis, axis=dim, tiled=True)]
    all_to_all x0 -> x1, starting transfers between devices: none -> 19.7 us  [rows_first(): lax.all_to_all(jnp.stack([both] * lax.axis_size(axis)), axis, 0, 0)]
    all_to_all x1, starting transfers between devices: 13.9 us -> 8.19 us  [sum_at_owner(): tiles = lax.all_to_all(in_blocks(array, dim, peers), axis, 0, 0, tiled=True)]
  transfers between devices with their start and end apart: 4 -> 4, of which waited for: 4 -> 3; matrix products, arithmetic and copies ran while one was open for 2% -> 1% of each run, Pallas kernels for 0% -> 0%
where the time goes in v1:
time: 405 us; the launch traced here: 404 us
  waiting for transfers between devices  259 us (64%)
  blocking collectives  63.6 us (16%)
  starting transfers between devices  32.3 us (8%)
  matrix products  22.1 us (5%)
  between operations  13.6 us (3%)
  other arithmetic  9.09 us (2%)
    all_gather x1, waiting for transfers between devices, sent_together(): out = lax.all_gather(both, axis, axis=dim, tiled=True)  226 us
    all_to_all x2, blocking collectives, sum_at_owner(): tiles = lax.all_to_all(in_blocks(array, dim, peers), axis, 0, 0, tiled=True)  42.4 us
    all_to_all x1, blocking collectives, sent_to_all(): lax.all_to_all(jnp.broadcast_to(array[None], (peers, *array.shape)), axis...  21.2 us
    all_to_all x1, starting transfers between devices, rows_first(): lax.all_to_all(jnp.stack([both] * lax.axis_size(axis)), axis, 0, 0)  19.7 us
    all_to_all x1, waiting for transfers between devices, sent_to_all(): lax.all_to_all(jnp.broadcast_to(array[None], (peers, *array.shape)), axis...  17.8 us
    all_to_all x1, waiting for transfers between devices, sum_at_owner(): tiles = lax.all_to_all(in_blocks(array, dim, peers), axis, 0, 0, tiled=True)  16 us
    dot_general x3, matrix products, reduce_rows(): jnp.dot(left_rows, right_matrix, preferred_element_type=jnp.float32)  14.8 us
    all_to_all x1, starting transfers between devices, sum_at_owner(): tiles = lax.all_to_all(in_blocks(array, dim, peers), axis, 0, 0, tiled=True)  8.19 us
  transfers between devices with their start and end apart: 4, of which 3 were waited for; matrix products, arithmetic and copies ran while one was open for 1% of the time, Pallas kernels for 0%

profile of v1, /device:TPU:1, one launch (start us, length us, event | category | flops | bytes accessed | tf_op | source)
XLA Modules:
  0.0 404.0 jit_solution(2548190443062991759)
XLA Ops:
  6.5 0.9 pad_maximum_fusion.1
  7.5 2.6 stack.2
  10.1 19.7 %all-to-all-start = ((bf16[64,32,960]{2,1,0:T(8,128)(2,1)}), bf16[64,32,960]{2,1,0:T(8,128)(2,1)}, u32[]{:S(2)}, u32[]{:S(2)}) async-start(bf16[64,32,960]{2,1,0:T(8,128)(2,1)} %stack.2), calls=%async_computation | async-start | bytes 8388608 | tf_op jit(solution)/shard_map/all_to_all | solution.py:44
  29.8 0.7 pad_maximum_fusion
  30.6 0.4 multiply_reduce_fusion
  31.0 225.6 %all-gather.2.cloned.1.call-done = bf16[2048,1408]{1,0:T(8,128)(2,1)} async-done(((bf16[32,1408]{1,0:T(8,128)(2,1)}), bf16[2048,1408]{1,0:T(8,128)(2,1)}) %all-gather.2.cloned.1.call-update) | async-done | bytes 5767184 | tf_op jit(solution)/shard_map/all_gather | solution.py:59
  256.6 3.1 fusion.10
  259.7 6.9 %fusion.12 = bf16[320,2048]{1,0:T(8,128)(2,1)} fusion(bf16[2048,960]{1,0:T(8,128)(2,1)} %bitcast.3, bf16[2048,1408]{1,0:T(8,128)(2,1)} %all-gather.2.cloned.1.call-done, f32[320,704]{1,0:T(8,128)S(1)} %fusion.10, f32[2048]{0:T(1024)S(1)} %bitcast.62, f32[320]{0:T(512)S(1)} %add_rsqrt_fusion, bf16[320,2048]{1,0:T(8,128)(2,1)S(1)} %copy-done.1), kind=kOutput, calls=%fused_computation.13 | convolution fusion | flops 1850122240 | bytes 9823488 | tf_op jit(solution)/shard_map/dot_general | solution.py:69
  266.6 8.2 %all-to-all-start.1 = ((bf16[8,40,2048]{2,1,0:T(8,128)(2,1)}), bf16[8,40,2048]{2,1,0:T(8,128)(2,1)S(1)}, u32[]{:S(2)}, u32[]{:S(2)}) async-start(bf16[8,40,2048]{2,1,0:T(8,128)(2,1)} %bitcast.49), calls=%async_computation.1 | async-start | bytes 2621440 | tf_op jit(solution)/shard_map/all_to_all | solution.py:17
  274.8 1.8 convert_element_type.82
  276.6 16.0 %all-to-all-done.1 = bf16[8,40,2048]{2,1,0:T(8,128)(2,1)S(1)} async-done(((bf16[8,40,2048]{2,1,0:T(8,128)(2,1)}), bf16[8,40,2048]{2,1,0:T(8,128)(2,1)S(1)}, u32[]{:S(2)}, u32[]{:S(2)}) %all-to-all-start.1) | async-done | bytes 1310752 | tf_op jit(solution)/shard_map/all_to_all | solution.py:17
  292.6 0.2 convert_reduce_fusion.2
  292.8 0.1 multiply_reduce_fusion.5
  292.9 1.2 multiply_reduce_fusion.4
  294.3 1.2 broadcast_in_dim.60
  295.5 4.4 %all-to-all-start.2 = ((bf16[8,40,2048]{2,1,0:T(8,128)(2,1)}), bf16[8,40,2048]{2,1,0:T(8,128)(2,1)S(1)}, u32[]{:S(2)}, u32[]{:S(2)}) async-start(bf16[8,40,2048]{2,1,0:T(8,128)(2,1)} %broadcast_in_dim.60), calls=%async_computation.2 | async-start | bytes 2621440 | tf_op jit(solution)/shard_map/all_to_all | solution.py:23
  300.0 17.8 %all-to-all-done.2 = bf16[8,40,2048]{2,1,0:T(8,128)(2,1)S(1)} async-done(((bf16[8,40,2048]{2,1,0:T(8,128)(2,1)}), bf16[8,40,2048]{2,1,0:T(8,128)(2,1)S(1)}, u32[]{:S(2)}, u32[]{:S(2)}) %all-to-all-start.2) | async-done | bytes 1310752 | tf_op jit(solution)/shard_map/all_to_all | solution.py:23
  317.7 1.8 convolution_convert_fusion.1
  319.7 1.7 subtract_convert_fusion
  321.4 0.1 fusion.43
  321.6 2.0 convolution_convert_fusion
  323.5 21.1 %all_to_all.30 = bf16[8,40,2048]{2,1,0:T(8,128)(2,1)S(1)} all-to-all(bf16[8,40,2048]{2,1,0:T(8,128)(2,1)S(1)} %bitcast.45), channel_id=1, replica_groups=mesh['fs'=64,'tp'=8] {'tp'}, dimensions={0} | all-to-all | bytes 2621440 | tf_op jit(solution)/shard_map/all_to_all | solution.py:17
  344.7 0.2 convert_reduce_fusion.1
  344.9 0.1 multiply_reduce_fusion.3
  345.0 0.2 multiply_reduce_fusion.2
  345.4 0.1 broadcast_in_dim.68
  345.5 21.2 %all_to_all.31 = bf16[8,40,2048]{2,1,0:T(8,128)(2,1)S(1)} all-to-all(bf16[8,40,2048]{2,1,0:T(8,128)(2,1)S(1)} %broadcast_in_dim.68), channel_id=1, replica_groups=mesh['fs'=64,'tp'=8] {'tp'}, dimensions={0} | all-to-all | bytes 2621440 | tf_op jit(solution)/shard_map/all_to_all | solution.py:23
  366.8 2.2 fusion.8
  368.9 5.9 %fusion.15 = bf16[320,2048]{1,0:T(8,128)(2,1)S(1)} fusion(bf16[2048,960]{1,0:T(8,128)(2,1)} %bitcast.3, bf16[320,2048]{1,0:T(8,128)(2,1)S(1)} %bitcast.51, bf16[2048,1408]{1,0:T(8,128)(2,1)} %all-gather.2.cloned.1.call-done, f32[320,704]{1,0:T(8,128)} %fusion.8), kind=kOutput, calls=%fused_computation.14 | convolution fusion | flops 1847500800 | bytes 9895936 | tf_op jit(solution)/shard_map/dot_general | solution.py:69
  374.8 21.2 %all_to_all.32 = bf16[8,40,2048]{2,1,0:T(8,128)(2,1)S(1)} all-to-all(bf16[8,40,2048]{2,1,0:T(8,128)(2,1)S(1)} %bitcast.52), channel_id=1, replica_groups=mesh['fs'=64,'tp'=8] {'tp'}, dimensions={0} | all-to-all | bytes 2621440 | tf_op jit(solution)/shard_map/all_to_all | solution.py:17
  396.1 0.2 convert_reduce_fusion
  396.4 0.8 add_convert_fusion
  (36 shorter events, 0.7 us)
Async XLA Ops:
  6.5 314.8 %copy-start = (bf16[1,128,128]{2,1,0:T(8,128)(2,1)S(1)}, bf16[1,128,128]{2,1,0:T(8,128)(2,1)}, u32[]{:S(2)}) copy-start(bf16[1,128,128]{2,1,0:T(8,128)(2,1)} %param.15) | copy-start | bytes 98308
  10.1 19.7 %copy-start.2 = (bf16[32,704]{1,0:T(8,128)(2,1)S(1)}, bf16[32,704]{1,0:T(8,128)(2,1)}, u32[]{:S(2)}) copy-start(bf16[32,704]{1,0:T(8,128)(2,1)} %param.11) | copy-start | bytes 135172
  10.1 19.8 %copy-start.3 = (bf16[32,704]{1,0:T(8,128)(2,1)S(1)}, bf16[32,704]{1,0:T(8,128)(2,1)}, u32[]{:S(2)}) copy-start(bf16[32,704]{1,0:T(8,128)(2,1)} %param.10) | copy-start | bytes 135172
  10.1 20.5 %copy-start.1 = (bf16[320,2048]{1,0:T(8,128)(2,1)S(1)}, bf16[320,2048]{1,0:T(8,128)(2,1)}, u32[]{:S(2)}) copy-start(bf16[320,2048]{1,0:T(8,128)(2,1)} %param.9) | copy-start | bytes 3932164
  10.1 20.9 %copy-start.4 = (f32[6,2048]{1,0:T(8,128)S(1)}, f32[6,2048]{1,0:T(8,128)}, u32[]{:S(2)}) copy-start(f32[6,2048]{1,0:T(8,128)} %param.17) | copy-start | bytes 147460
  10.1 249.6 %all-to-all-start = ((bf16[64,32,960]{2,1,0:T(8,128)(2,1)}), bf16[64,32,960]{2,1,0:T(8,128)(2,1)}, u32[]{:S(2)}, u32[]{:S(2)}) async-start(bf16[64,32,960]{2,1,0:T(8,128)(2,1)} %stack.2), calls=%async_computation | async-start | bytes 8388608 | tf_op jit(solution)/shard_map/all_to_all | solution.py:44
  29.8 226.8 %all-gather.2.cloned.1.call-start = ((), (), s32[]{:S(2)}) async-start(), calls=%async_computation.6 | async-start | bytes 5857280 | tf_op jit(solution)/shard_map/all_gather | solution.py:59
  266.6 26.0 %all-to-all-start.1 = ((bf16[8,40,2048]{2,1,0:T(8,128)(2,1)}), bf16[8,40,2048]{2,1,0:T(8,128)(2,1)S(1)}, u32[]{:S(2)}, u32[]{:S(2)}) async-start(bf16[8,40,2048]{2,1,0:T(8,128)(2,1)} %bitcast.49), calls=%async_computation.1 | async-start | bytes 2621440 | tf_op jit(solution)/shard_map/all_to_all | solution.py:17
  292.9 7.0 %copy-start.5 = (bf16[128]{0:T(256)(128)(2,1)S(1)}, bf16[128]{0:T(256)(128)(2,1)}, u32[]{:S(2)}) copy-start(bf16[128]{0:T(256)(128)(2,1)} %param.16) | copy-start | bytes 772
  295.5 22.2 %all-to-all-start.2 = ((bf16[8,40,2048]{2,1,0:T(8,128)(2,1)}), bf16[8,40,2048]{2,1,0:T(8,128)(2,1)S(1)}, u32[]{:S(2)}, u32[]{:S(2)}) async-start(bf16[8,40,2048]{2,1,0:T(8,128)(2,1)} %broadcast_in_dim.60), calls=%async_computation.2 | async-start | bytes 2621440 | tf_op jit(solution)/shard_map/all_to_all | solution.py:23
  321.6 45.2 %slice-start = ((s8[5767168]{0:T(1024)(128)(4,1)}), s8[4194304]{0:T(1024)(128)(4,1)S(1)}, s32[]{:S(2)}) async-start(s8[5767168]{0:T(1024)(128)(4,1)} %bitcast.63), calls=%async_computation.7 | async-start | bytes 8388608
  344.7 22.1 %slice-start.1 = ((s8[5767168]{0:T(1024)(128)(4,1)}), s8[1572864]{0:T(1024)(128)(4,1)S(1)}, s32[]{:S(2)}) async-start(s8[5767168]{0:T(1024)(128)(4,1)} %bitcast.63), calls=%async_computation.8 | async-start | bytes 3145728
Sparse Core Ops, SparseCore 0:
  33.5 222.9 all-gather.1
